TPU v7x, 32 devices: a whole 2x2x4 slice. The times are simulated.
32 devices in a mesh: grp: 2 (over y), fs: 4 (over z), tp: 4 (over x, core).
Axes of the slice: x: 2, y: 2, z: 4, core: 2. Of those that a mesh axis runs over, the one named last changes fastest.
Arguments:
- tokens: bfloat16 [2048, 2048], P(('grp', 'fs')), parts along dimension 0, may hold values from -6 to 6
- norm_gain: float32 [2048], P('fs'), may hold values from 0.1 to 1.9
- gate_master: float32 [4, 2048, 1024], P(None, 'fs', 'tp'), may hold values from -0.125 to 0.125
- up_master: float32 [4, 2048, 1024], P(None, 'fs', 'tp'), may hold values from -0.125 to 0.125
- chosen: int32 [2048, 2], P(('grp', 'fs')), parts along dimension 0, may hold values from 0 to 3, all different within a row; in each aligned block of 256 rows (0 to 255, 256 to 511, ...) at most 256 rows name the same one
- affinity: float32 [2048, 2], P(('grp', 'fs')), parts along dimension 0, may hold values from 0.05 to 1
Outputs:
- gate_served: bfloat16 [8, 2048, 1024], P(('grp', 'fs'), None, 'tp'), parts along dimension 0
- up_served: bfloat16 [8, 2048, 1024], P(('grp', 'fs'), None, 'tp'), parts along dimension 0
- hidden: bfloat16 [2048, 2, 1024], P(('grp', 'fs'), None, 'tp'), parts along dimension 0
There are 2 independent parts, one for each index of `grp`. A program takes and returns all parts, laid end to end along the dimension named above; an argument that names none is the same for every part. Nothing has to cross between parts.
Inputs may be any that keep to these rules, and one draw needn't show every extreme that they name: Among the rows of one index of fs (256 tokens, all their choices) no expert is chosen more than 256 times, a bound that some block reaches; the choices of one token differ.
All inputs are finite; a program needn't handle non-finite values.
Results may differ from a plain program's by a relative error of at most 0.023.
Values may be sent and summed in bfloat16 or wider, within the bound.
A program may use at most 64 MiB of HBM per device.

v0:
```python
import functools

import jax
import jax.numpy as jnp
from jax import lax
from jax.experimental import pallas as pl
from jax.experimental.pallas import tpu as pltpu
from jax.sharding import PartitionSpec as P

MESH = pl.DeviceIdType.MESH
CHUNKS = 2
PIECES = 4
HALVES = 2


def routed(tokens, norm_gain, gate_master, up_master, chosen, affinity):
    folded_gate = (gate_master * norm_gain[None, :, None]).astype(jnp.bfloat16)
    folded_up = (up_master * norm_gain[None, :, None]).astype(jnp.bfloat16)
    new_gate, new_up = (
        lax.all_to_all(folded_gate, "fs", split_axis=0, concat_axis=1, tiled=True),
        lax.all_to_all(folded_up, "fs", split_axis=0, concat_axis=1, tiled=True),
    )
    experts_all = gate_master.shape[0]
    tok_rows, width = tokens.shape
    top = chosen.shape[1]
    capacity = tok_rows * top * 2 // experts_all
    local = new_gate.shape[0]
    xfloat = tokens.astype(jnp.float32)
    scale = lax.rsqrt(jnp.mean(xfloat * xfloat, axis=-1) + 1e-06)
    share = affinity / jnp.sum(affinity, axis=-1, keepdims=True)
    flat_e = chosen.reshape(-1)
    onehot = (flat_e[:, None] == jnp.arange(experts_all, dtype=jnp.int32)[None, :]).astype(
        jnp.int32
    )
    slot = jnp.sum((jnp.cumsum(onehot, axis=0) - onehot) * onehot, axis=1)
    target = flat_e * capacity + slot
    owner = jnp.repeat(jnp.arange(tok_rows, dtype=jnp.int32), top)
    total = experts_all * capacity
    scale_buf = (
        jnp.zeros((total,), jnp.float32).at[target].set(scale[owner]).reshape(experts_all, capacity)
    )
    share_buf = (
        jnp.zeros((total,), jnp.float32)
        .at[target]
        .set(share.reshape(-1))
        .reshape(experts_all, capacity)
    )
    narrow = width // lax.axis_size("tp")
    own_cols = lax.dynamic_slice_in_dim(tokens, lax.axis_index("tp") * narrow, narrow, 1)
    row_buf = jnp.zeros((total, narrow), jnp.bfloat16).at[target].set(own_cols[owner])
    row_buf = row_buf.reshape(experts_all, capacity, narrow)
    got_rows, got_scale, got_share = (
        lax.all_to_all(row_buf, "fs", split_axis=0, concat_axis=0, tiled=True),
        lax.all_to_all(
            scale_buf.astype(jnp.bfloat16), "fs", split_axis=0, concat_axis=0, tiled=True
        ).astype(scale_buf.dtype),
        lax.all_to_all(
            share_buf.astype(jnp.bfloat16), "fs", split_axis=0, concat_axis=0, tiled=True
        ).astype(share_buf.dtype),
    )
    sources = got_rows.shape[0] // local
    got_rows = got_rows.reshape(sources, local, capacity, narrow)
    piece = lax.all_gather(got_rows, "tp", axis=3, tiled=True)
    gate = jnp.einsum("secd,edf->secf", piece, new_gate, preferred_element_type=jnp.float32)
    up = jnp.einsum("secd,edf->secf", piece, new_up, preferred_element_type=jnp.float32)
    factor = got_scale.reshape(sources, local, capacity)[..., None]
    weight = got_share.reshape(sources, local, capacity)[..., None]
    gate = gate * factor
    up = up * factor
    hidden_rows = (weight * jax.nn.silu(gate) * up).astype(jnp.bfloat16)
    hidden_rows = hidden_rows.reshape(sources * local, capacity, hidden_rows.shape[3])
    back = lax.all_to_all(hidden_rows, "fs", split_axis=0, concat_axis=0, tiled=True)
    picked = back.reshape(total, back.shape[2])[target].reshape(tok_rows, top, back.shape[2])
    return (new_gate, new_up, picked)


def dense_kernel(
    n, nt, width,
    tok_hbm, gain_ref, gate_hbm, up_hbm, chosen_ref, aff_ref,
    gate_out, up_out, hid_out,
    tok, wf, own, wsend, W, scale, hs, hr,
    ls_tok, ls_w, ls_own, os,
    ss_tz, ss_tx, ss_tm, rs_tok, ss_w, rs_w, ss_y, ss_h, rs_h,
):
    g, z, t = lax.axis_index("grp"), lax.axis_index("fs"), lax.axis_index("tp")
    depth, fcols = wf.shape[1], wf.shape[2]
    fc = fcols // CHUNKS
    mate = t + 1 - 2 * lax.rem(t, 2)
    xq = lax.rem(t + 2, nt)
    xmate = lax.rem(mate + 2, nt)
    rows = tok.shape[2]

    def remote(src, dst, ssem, rsem, **dev):
        return pltpu.make_async_remote_copy(
            src_ref=src, dst_ref=dst, send_sem=ssem, recv_sem=rsem, device_id=dev, device_id_type=MESH
        )

    def tok_load(q):
        return pltpu.make_async_copy(
            tok_hbm.at[:, pl.ds(pl.multiple_of(q * depth, depth), depth)], tok.at[z, q], ls_tok.at[q]
        )

    tok_load(t).start()
    for off in range(1, n):
        e = lax.rem(z + off, n)

        @pl.when(g == 0)
        def _():
            pltpu.make_async_copy(gate_hbm.at[e], wf.at[e], ls_w.at[e]).start()

        @pl.when(g != 0)
        def _():
            pltpu.make_async_copy(up_hbm.at[e], wf.at[e], ls_w.at[e]).start()

    own_loads = [
        pltpu.make_async_copy(gate_hbm.at[z], own.at[0], ls_own.at[0]),
        pltpu.make_async_copy(up_hbm.at[z], own.at[1], ls_own.at[1]),
    ]
    for copy in own_loads:
        copy.start()
    for off in range(1, nt):
        tok_load(lax.rem(t + off, nt)).start()

    barrier = pltpu.get_barrier_semaphore()
    for off in range(1, n):
        pl.semaphore_signal(barrier, 1, device_id={"fs": lax.rem(z + off, n)}, device_id_type=MESH)
    pl.semaphore_signal(barrier, 1, device_id={"grp": 1 - g}, device_id_type=MESH)
    pl.semaphore_signal(barrier, 1, device_id={"tp": mate}, device_id_type=MESH)
    pl.semaphore_signal(barrier, 1, device_id={"tp": xq}, device_id_type=MESH)
    pl.semaphore_wait(barrier, n + 2)

    def block(s, q, h):
        return tok.at[s, q, pl.ds(h * (rows // HALVES), rows // HALVES)]

    def tz(s, step, h):
        ref = block(s, t, h)
        return remote(ref, ref, ss_tz.at[s, (step + 1) // 2, h], rs_tok.at[s, t, h], fs=z + step)

    def tx(s, h):
        ref = block(s, t, h)
        return remote(ref, ref, ss_tx.at[s, h], rs_tok.at[s, t, h], tp=xq)

    def tm(s, q, i, h):
        ref = block(s, q, h)
        return remote(ref, ref, ss_tm.at[s, i, h], rs_tok.at[s, q, h], tp=mate)

    def tok_wait(s, q, h):
        ref = block(s, q, h)
        remote(ref, ref, ss_tx.at[s, h], rs_tok.at[s, q, h], tp=mate).wait_recv()

    def sides(d, fn):
        for sign in (1, -1):
            s = z + sign * d

            @pl.when((s >= 0) & (s < n))
            def _():
                fn(s, sign)

    tok_load(t).wait()
    for h in range(HALVES):
        sides(1, lambda s, sign: tz(z, sign, h).start())

    gcol = jnp.transpose(jnp.broadcast_to(gain_ref[...], (128, depth)))
    gcol = jnp.concatenate([gcol] * (fc // 128), axis=1) if fc > 128 else gcol

    def fold(s, sign):
        pltpu.make_async_copy(gate_hbm.at[s], wf.at[s], ls_w.at[s]).wait()
        for c in range(CHUNKS):
            wsend[s, c] = (wf[s, :, c * fc : (c + 1) * fc] * gcol).astype(jnp.bfloat16)

    def lanes(m):
        return pl.ds(pl.multiple_of(m * fc, fc), fc)

    def part(p):
        return pl.ds(p * (depth // PIECES), depth // PIECES)

    def wcopy(c, p, to):
        src, dst = wsend.at[to, c, part(p)], W.at[z, c, part(p), lanes(g)]
        return remote(src, dst, ss_w.at[c, p, to], rs_w.at[g, c, p, z], fs=to)

    def send_weights(c):
        for p in range(PIECES):
            for d in range(n - 1, 0, -1):
                sides(d, lambda s, sign: wcopy(c, p, s).start())

    for d in range(n - 1, 0, -1):
        sides(d, fold)
    at_end = (z == 0) | (z == n - 1)


    def out_copy(m, c, s):
        ref = (gate_out, up_out)[m]
        return pltpu.make_async_copy(
            W.at[s, c, :, pl.ds(m * fc, fc)],
            ref.at[0, pl.ds(pl.multiple_of(s * depth, depth), depth), pl.ds(c * fc, fc)],
            os.at[m, c, s],
        )

    for m in range(2):
        own_loads[m].wait()
        for c in range(CHUNKS):
            W[z, c, :, m * fc : (m + 1) * fc] = (own[m, :, c * fc : (c + 1) * fc] * gcol).astype(jnp.bfloat16)

    def arrive_all(d):
        for h in range(HALVES):

            def arrive(s, sign):
                tok_wait(s, t, h)
                nxt = z - sign

                @pl.when((nxt >= 0) & (nxt < n))
                def _():
                    tz(s, -sign, h).start()

                tx(s, h).start()
                tm(s, t, 0, h).start()

            sides(d, arrive)

    def xrelay(s, sign):
        for h in range(HALVES):
            tok_wait(s, xq, h)
            tm(s, xq, 1, h).start()

    def ycopy(c, p, s):
        ref = W.at[s, c, part(p), lanes(g)]
        return remote(ref, ref, ss_y.at[c, p, s], rs_w.at[g, c, p, s], grp=1 - g)

    def yforward(c):
        for p in range(PIECES):

            def one(s, sign):
                src, dst = wsend.at[s, c, part(p)], W.at[s, c, part(p), lanes(g)]
                remote(src, dst, ss_w.at[c, p, s], rs_w.at[g, c, p, s], fs=s).wait_recv()
                ycopy(c, p, s).start()

            for d in range(n - 1, 0, -1):
                sides(d, one)

    def ywait(c):
        def one(s, sign):
            o = 1 - g
            for p in range(PIECES):
                ref = W.at[s, c, part(p), lanes(o)]
                remote(ref, ref, ss_y.at[c, p, s], rs_w.at[o, c, p, s], grp=o).wait_recv()

        for d in range(1, n):
            sides(d, one)
        for s in range(n):
            for m in range(2):
                out_copy(m, c, s).start()

    def hcopy(c, to):
        return remote(hs.at[to, c], hr.at[z, c], ss_h.at[c, to], rs_h.at[c, z], fs=to)

    def sumsq(s):
        part = jnp.zeros((rows, 128), jnp.float32)
        for q in range(nt):
            for i in range(depth // 128):
                x = tok[s, q, :, i * 128 : (i + 1) * 128].astype(jnp.float32)
                part = part + x * x
        total = jnp.sum(part, axis=-1, keepdims=True)
        scale[s] = jnp.broadcast_to(lax.rsqrt(total / width + 1e-06), (rows, fc))

    def compute(c):
        def body(i, carry):
            s = lax.rem(z + 1 + i, n)
            acc = jnp.dot(tok[s, 0], W[0, c], preferred_element_type=jnp.float32)
            for q in range(1, nt):
                acc = acc + jnp.dot(tok[s, q], W[q, c], preferred_element_type=jnp.float32)
            gate = acc[:, :fc] * scale[s]
            up = acc[:, fc:] * scale[s]
            h = (gate / (1.0 + jnp.exp(-gate)) * up).astype(jnp.bfloat16)

            @pl.when(s != z)
            def _():
                hs[s, c] = h
                hcopy(c, s).start()

            @pl.when(s == z)
            def _():
                hr[z, c] = h

            return carry

        lax.fori_loop(0, n, body, 0)

    arrive_all(1)

    arrive_all(2)
    send_weights(0)
    sides(1, xrelay)
    for d in range(3, n):
        arrive_all(d)
    for c in range(1, CHUNKS):
        send_weights(c)
    yforward(0)
    for d in range(2, n):
        sides(d, xrelay)
    for off in range(1, nt):
        tok_load(lax.rem(t + off, nt)).wait()
    sumsq(z)

    def rest(s, sign):
        for h in range(HALVES):
            tok_wait(s, mate, h)
            tok_wait(s, xmate, h)
        sumsq(s)

    for d in range(1, n):
        sides(d, rest)
    for c in range(1, CHUNKS):
        yforward(c)
    for c in range(CHUNKS):
        ywait(c)
        compute(c)

    aff = aff_ref[...]
    share = aff / jnp.sum(aff, axis=0, keepdims=True)
    top = aff.shape[0]

    def column(row):
        col = jnp.transpose(jnp.broadcast_to(row, (128, rows)))
        return jnp.concatenate([col] * (fc // 128), axis=1) if fc > 128 else col

    shares = [column(share[k : k + 1, :]) for k in range(top)]
    names = [column(chosen_ref[k : k + 1, :].astype(jnp.float32)) for k in range(top)]
    for c in range(CHUNKS):
        for off in range(1, n):
            s = lax.rem(z + off, n)
            remote(hs.at[s, c], hr.at[s, c], ss_h.at[c, s], rs_h.at[c, s], fs=s).wait_recv()
        for k in range(top):
            picked = jnp.zeros((rows, fc), jnp.float32)
            for e in range(n):
                picked = jnp.where(names[k] == e, hr[e, c].astype(jnp.float32), picked)
            hid_out[:, k * fcols + c * fc : k * fcols + (c + 1) * fc] = (
                picked * shares[k]
            ).astype(jnp.bfloat16)

    for h in range(HALVES):
        sides(1, lambda s, sign: tz(z, sign, h).wait_send())

    def drain(s, sign):
        nxt = z - sign

        for h in range(HALVES):

            @pl.when((nxt >= 0) & (nxt < n))
            def _():
                tz(s, -sign, h).wait_send()

            tx(s, h).wait_send()
            tm(s, t, 0, h).wait_send()
            tm(s, xq, 1, h).wait_send()
        for c in range(CHUNKS):
            for p in range(PIECES):
                wcopy(c, p, s).wait_send()
                ycopy(c, p, s).wait_send()
            hcopy(c, s).wait_send()

    for d in range(1, n):
        sides(d, drain)
    for c in range(CHUNKS):
        for s in range(n):
            for m in range(2):
                out_copy(m, c, s).wait()


def dense(tokens, norm_gain, gate_master, up_master, chosen, affinity):
    n, nt = lax.axis_size("fs"), lax.axis_size("tp")
    rows, width = tokens.shape
    experts, depth, fcols = gate_master.shape
    top = chosen.shape[1]
    fc = fcols // CHUNKS
    bf, f32 = jnp.bfloat16, jnp.float32
    dma = pltpu.SemaphoreType.DMA
    any_spec = pl.BlockSpec(memory_space=pl.ANY)
    hbm = pl.BlockSpec(memory_space=pltpu.HBM)
    vmem = pl.BlockSpec(memory_space=pltpu.VMEM)
    gate, up, hid = pl.pallas_call(
        functools.partial(dense_kernel, n, nt, width),
        out_shape=(
            jax.ShapeDtypeStruct((1, width, fcols), bf),
            jax.ShapeDtypeStruct((1, width, fcols), bf),
            jax.ShapeDtypeStruct((rows, top * fcols), bf),
        ),
        in_specs=[hbm, vmem, hbm, hbm, vmem, vmem],
        out_specs=(any_spec, any_spec, vmem),
        scratch_shapes=[
            pltpu.VMEM((n, nt, rows, depth), bf),
            pltpu.VMEM((n, depth, fcols), f32),
            pltpu.VMEM((2, depth, fcols), f32),
            pltpu.VMEM((n, CHUNKS, depth, fc), bf),
            pltpu.VMEM((n, CHUNKS, depth, 2 * fc), bf),
            pltpu.VMEM((n, rows, fc), f32),
            pltpu.VMEM((n, CHUNKS, rows, fc), bf),
            pltpu.VMEM((n, CHUNKS, rows, fc), bf),
            dma((nt,)),
            dma((n,)),
            dma((2,)),
            dma((2, CHUNKS, n)),
            dma((n, 2, HALVES)),
            dma((n, HALVES)),
            dma((n, 2, HALVES)),
            dma((n, nt, HALVES)),
            dma((CHUNKS, PIECES, n)),
            dma((2, CHUNKS, PIECES, n)),
            dma((CHUNKS, PIECES, n)),
            dma((CHUNKS, n)),
            dma((CHUNKS, n)),
        ],
        compiler_params=pltpu.CompilerParams(
            collective_id=0, has_side_effects=True, vmem_limit_bytes=51 * 1024 * 1024
        ),
    )(tokens, norm_gain.reshape(1, depth), gate_master, up_master, chosen.T, affinity.T)
    return gate, up, hid.reshape(rows, top, fcols)


def on_device(tokens, norm_gain, gate_master, up_master, chosen, affinity):
    n, nt = lax.axis_size("fs"), lax.axis_size("tp")
    experts, depth, fcols = gate_master.shape
    rows, width = tokens.shape
    capacity = rows * chosen.shape[1] * 2 // experts
    fits = (
        experts == n
        and capacity >= rows
        and n >= 3
        and nt == 4
        and lax.axis_size("grp") == 2
        and width == nt * depth
        and fcols % (CHUNKS * 128) == 0
    )
    run = dense if fits else routed
    return run(tokens, norm_gain, gate_master, up_master, chosen, affinity)


def solution(mesh):
    return jax.shard_map(
        on_device,
        mesh=mesh,
        in_specs=(
            P(("grp", "fs"), None),
            P("fs"),
            P(None, "fs", "tp"),
            P(None, "fs", "tp"),
            P(("grp", "fs"), None),
            P(("grp", "fs"), None),
        ),
        out_specs=(
            P(("grp", "fs"), None, "tp"),
            P(("grp", "fs"), None, "tp"),
            P(("grp", "fs"), None, "tp"),
        ),
        check_vma=False,
    )
```

profile of v0, /device:TPU:0, one launch (start us, length us, event | category | flops | bytes accessed | tf_op | source)
XLA Modules:
  0.0 61.5 jit_solution(10880582541157975687)
XLA Ops:
  0.6 0.0 copy-start
  0.6 0.7 %copy-done = f32[512]{0:T(512)S(1)} copy-done((f32[512]{0:T(512)S(1)}, f32[512]{0:T(512)}, u32[]{:S(2)}) %copy-start) | copy-done | bytes 2072
  1.3 0.0 copy-start.1
  1.3 0.7 %copy-done.1 = s32[256,2]{0,1:T(2,128)S(1)} copy-done((s32[256,2]{0,1:T(2,128)S(1)}, s32[256,2]{0,1:T(2,128)}, u32[]{:S(2)}) %copy-start.1) | copy-done | bytes 2072
  2.0 0.0 copy-start.2
  2.0 0.7 %copy-done.2 = f32[256,2]{0,1:T(2,128)S(1)} copy-done((f32[256,2]{0,1:T(2,128)S(1)}, f32[256,2]{0,1:T(2,128)}, u32[]{:S(2)}) %copy-start.2) | copy-done | bytes 2072
  2.7 56.1 %shard_map.85 = (bf16[1,2048,256]{2,1,0:T(8,128)(2,1)S(1)}, bf16[1,2048,256]{2,1,0:T(8,128)(2,1)S(1)}, bf16[256,512]{1,0:T(8,128)(2,1)S(1)}) custom-call(bf16[256,2048]{1,0:T(8,128)(2,1)} %tok_hbm.1, f32[1,512]{1,0:T(1,128)S(1)} %bitcast.3, f32[4,512,256]{2,1,0:T(8,128)} %gate_hbm.1, f32[4,512,256]{2,1,0:T(8,128)} %up_hbm.1, s32[2,256]{1,0:T(2,128)S(1)} %bitcast.4, ...), custom_call_target="tpu_custom_call" | custom-call | tf_op jit(solution)/shard_map/pallas_call | solution.py:380
  58.8 0.8 %reshape.13 = bf16[256,2,256]{2,1,0:T(2,128)(2,1)} reshape(bf16[256,512]{1,0:T(8,128)(2,1)S(1)} %get-tuple-element.8) | data formatting | bytes 524288 | tf_op jit(solution)/shard_map/reshape | solution.py:416
  59.5 1.0 %copy.11 = bf16[1,2048,256]{2,1,0:T(8,128)(2,1)} copy(bf16[1,2048,256]{2,1,0:T(8,128)(2,1)S(1)} %get-tuple-element.12) | data formatting | bytes 2097152
  60.5 1.0 %copy.12 = bf16[1,2048,256]{2,1,0:T(8,128)(2,1)} copy(bf16[1,2048,256]{2,1,0:T(8,128)(2,1)S(1)} %get-tuple-element.13) | data formatting | bytes 2097152
Async XLA Ops:
  0.6 0.7 %copy-start = (f32[512]{0:T(512)S(1)}, f32[512]{0:T(512)}, u32[]{:S(2)}) copy-start(f32[512]{0:T(512)} %param.7) | copy-start | bytes 6148
  1.3 0.7 %copy-start.1 = (s32[256,2]{0,1:T(2,128)S(1)}, s32[256,2]{0,1:T(2,128)}, u32[]{:S(2)}) copy-start(s32[256,2]{0,1:T(2,128)} %param.10) | copy-start | bytes 6148
  2.0 0.7 %copy-start.2 = (f32[256,2]{0,1:T(2,128)S(1)}, f32[256,2]{0,1:T(2,128)}, u32[]{:S(2)}) copy-start(f32[256,2]{0,1:T(2,128)} %param.11) | copy-start | bytes 6148
where the time goes:
time: 61.7 us; the launch traced here: 61.5 us
  Pallas kernels  56.1 us (91%)
  local copies, waits for them, and re-layouts  4.74 us (8%)
  between operations  0.65 us (1%)
    pallas_call x1, Pallas kernels, dense(): pl.pallas_call(functools.partial(dense_kernel, n, nt, width), out_shape=(...  56.1 us
    unnamed x8, local copies, waits for them, and re-layouts  3.98 us

commit v1 on v0

v1 whole, which is shorter than its diff:
```python
import functools

import jax
import jax.numpy as jnp
from jax import lax
from jax.experimental import pallas as pl
from jax.experimental.pallas import tpu as pltpu
from jax.sharding import PartitionSpec as P

MESH = pl.DeviceIdType.MESH
CHUNKS = 2
HALVES = 2


def routed(tokens, norm_gain, gate_master, up_master, chosen, affinity):
    folded_gate = (gate_master * norm_gain[None, :, None]).astype(jnp.bfloat16)
    folded_up = (up_master * norm_gain[None, :, None]).astype(jnp.bfloat16)
    new_gate, new_up = (
        lax.all_to_all(folded_gate, "fs", split_axis=0, concat_axis=1, tiled=True),
        lax.all_to_all(folded_up, "fs", split_axis=0, concat_axis=1, tiled=True),
    )
    experts_all = gate_master.shape[0]
    tok_rows, width = tokens.shape
    top = chosen.shape[1]
    capacity = tok_rows * top * 2 // experts_all
    local = new_gate.shape[0]
    xfloat = tokens.astype(jnp.float32)
    scale = lax.rsqrt(jnp.mean(xfloat * xfloat, axis=-1) + 1e-06)
    share = affinity / jnp.sum(affinity, axis=-1, keepdims=True)
    flat_e = chosen.reshape(-1)
    onehot = (flat_e[:, None] == jnp.arange(experts_all, dtype=jnp.int32)[None, :]).astype(
        jnp.int32
    )
    slot = jnp.sum((jnp.cumsum(onehot, axis=0) - onehot) * onehot, axis=1)
    target = flat_e * capacity + slot
    owner = jnp.repeat(jnp.arange(tok_rows, dtype=jnp.int32), top)
    total = experts_all * capacity
    scale_buf = (
        jnp.zeros((total,), jnp.float32).at[target].set(scale[owner]).reshape(experts_all, capacity)
    )
    share_buf = (
        jnp.zeros((total,), jnp.float32)
        .at[target]
        .set(share.reshape(-1))
        .reshape(experts_all, capacity)
    )
    narrow = width // lax.axis_size("tp")
    own_cols = lax.dynamic_slice_in_dim(tokens, lax.axis_index("tp") * narrow, narrow, 1)
    row_buf = jnp.zeros((total, narrow), jnp.bfloat16).at[target].set(own_cols[owner])
    row_buf = row_buf.reshape(experts_all, capacity, narrow)
    got_rows, got_scale, got_share = (
        lax.all_to_all(row_buf, "fs", split_axis=0, concat_axis=0, tiled=True),
        lax.all_to_all(
            scale_buf.astype(jnp.bfloat16), "fs", split_axis=0, concat_axis=0, tiled=True
        ).astype(scale_buf.dtype),
        lax.all_to_all(
            share_buf.astype(jnp.bfloat16), "fs", split_axis=0, concat_axis=0, tiled=True
        ).astype(share_buf.dtype),
    )
    sources = got_rows.shape[0] // local
    got_rows = got_rows.reshape(sources, local, capacity, narrow)
    piece = lax.all_gather(got_rows, "tp", axis=3, tiled=True)
    gate = jnp.einsum("secd,edf->secf", piece, new_gate, preferred_element_type=jnp.float32)
    up = jnp.einsum("secd,edf->secf", piece, new_up, preferred_element_type=jnp.float32)
    factor = got_scale.reshape(sources, local, capacity)[..., None]
    weight = got_share.reshape(sources, local, capacity)[..., None]
    gate = gate * factor
    up = up * factor
    hidden_rows = (weight * jax.nn.silu(gate) * up).astype(jnp.bfloat16)
    hidden_rows = hidden_rows.reshape(sources * local, capacity, hidden_rows.shape[3])
    back = lax.all_to_all(hidden_rows, "fs", split_axis=0, concat_axis=0, tiled=True)
    picked = back.reshape(total, back.shape[2])[target].reshape(tok_rows, top, back.shape[2])
    return (new_gate, new_up, picked)


def dense_kernel(
    n, nt, width,
    tok_hbm, gain_hbm, gate_hbm, up_hbm, chosen_hbm, aff_hbm,
    served, hid_out,
    tok, wf, own, wsend, scale, hs, hr, gain, names_in, aff_in,
    ls_own_tok, ls_tok, ls_w, ls_own, ls_gain, ls_names, ls_aff,
    ss_tok, ss_w, ss_y, ss_h, rs_tz, rs_tx, rs_tm, rs_w, rs_y, rs_h, far,
):
    g, z, t = lax.axis_index("grp"), lax.axis_index("fs"), lax.axis_index("tp")
    depth, fcols = wf.shape[1], wf.shape[2]
    fc = fcols // CHUNKS
    mate = t + 1 - 2 * lax.rem(t, 2)
    xq = lax.rem(t + 2, nt)
    rows = tok.shape[1]
    has_up, has_dn = z + 1 < n, z > 0
    at_end = (z == 0) | (z == n - 1)

    def remote(src, dst, ssem, rsem, **dev):
        return pltpu.make_async_remote_copy(
            src_ref=src, dst_ref=dst, send_sem=ssem, recv_sem=rsem, device_id=dev, device_id_type=MESH
        )

    def local(src, dst, sem):
        return pltpu.make_async_copy(src, dst, sem)

    def signal(sem, **dev):
        pl.semaphore_signal(sem, 1, device_id=dev, device_id_type=MESH)

    barrier = pltpu.get_barrier_semaphore()
    for there, step in ((has_up, 1), (has_dn, -1)):

        @pl.when(there)
        def _():
            signal(barrier, fs=z + step)

    signal(barrier, grp=1 - g)
    signal(barrier, tp=mate)
    signal(barrier, tp=xq)

    def tok_load(q, sem):
        return local(
            tok_hbm.at[:, pl.ds(pl.multiple_of(q * depth, depth), depth)], tok.at[z * nt + q], sem
        )

    own_load = tok_load(t, ls_own_tok)
    own_load.start()
    small_loads = (
        local(gain_hbm, gain, ls_gain),
        local(chosen_hbm, names_in, ls_names),
        local(aff_hbm, aff_in, ls_aff),
    )
    small_loads[0].start()
    for off in range(1, n):
        e = lax.rem(z + off, n)

        @pl.when(g == 0)
        def _():
            local(gate_hbm.at[e], wf.at[off - 1], ls_w).start()

        @pl.when(g != 0)
        def _():
            local(up_hbm.at[e], wf.at[off - 1], ls_w).start()

    for m, ref in enumerate((gate_hbm, up_hbm)):
        local(ref.at[z], own.at[m], ls_own).start()
    for off in range(1, nt):
        tok_load(lax.rem(t + off, nt), ls_tok).start()
    for copy in small_loads[1:]:
        copy.start()

    half = rows // HALVES

    def block(s, q, h):
        return tok.at[s * nt + q, pl.ds(h * half, half)]

    def tz(s, step, h):
        ref = block(s, t, h)
        return remote(ref, ref, ss_tok, rs_tz.at[s, h], fs=z + step)

    def tx(s, h):
        ref = block(s, t, h)
        return remote(ref, ref, ss_tok, rs_tx.at[s, h], tp=xq)

    def tm(s, q, h):
        ref = block(s, q, h)
        return remote(ref, ref, ss_tok, rs_tm.at[s], tp=mate)

    def sides(d, fn):
        for sign in (1, -1):
            s = z + sign * d

            @pl.when((s >= 0) & (s < n))
            def _():
                fn(s, sign)

    own_load.wait()
    pl.semaphore_wait(barrier, 5 - jnp.where(at_end, 1, 0))

    for h in range(HALVES):
        sides(1, lambda s, sign: tz(z, sign, h).start())

    @pl.when(has_up & has_dn)
    def _():
        signal(far.at[0, 0], fs=z - 1)
        signal(far.at[1, 0], fs=z + 1)

    def slot(s):
        return lax.rem(s - z + n, n) - 1

    small_loads[0].wait()
    gcol = jnp.transpose(jnp.broadcast_to(gain[...], (128, depth)))
    gcol = jnp.concatenate([gcol] * (fc // 128), axis=1) if fc > 128 else gcol
    local(gate_hbm.at[pl.ds(0, n - 1)], wf, ls_w).wait()
    for k in range(n - 1):
        for c in range(CHUNKS):
            wsend[k, c] = (wf[k, :, c * fc : (c + 1) * fc] * gcol).astype(jnp.bfloat16)

    def hears(k, others, way, there, step):
        @pl.when(k < others)
        def _():
            pl.semaphore_wait(far.at[way, k], 1)
            if k + 1 < n - 2:

                @pl.when(there)
                def _():
                    signal(far.at[way, k + 1], fs=z + step)

    for k in range(n - 2):
        hears(k, n - 2 - z, 0, has_dn, -1)
        hears(k, z - 1, 1, has_up, 1)

    def part(s, p):
        size = depth // n
        return pl.ds(pl.multiple_of(s * depth + p * size, size), size)

    def strip(m, s, c, p):
        return served.at[m, part(s, p), pl.ds(c * fc, fc)]

    def wcopy(c, p, to):
        src = wsend.at[slot(to), c, part(0, p)]
        return remote(src, strip(g, z, c, p), ss_w, rs_w.at[c, p, z], fs=to)

    def send_weights(c, p, distances):
        for d in distances:
            sides(d, lambda s, sign: wcopy(c, p, s).start())

    @pl.when(at_end)
    def _():
        for c in range(CHUNKS):
            for p in range(n):
                send_weights(c, p, (1,))

    local(gate_hbm.at[pl.ds(0, 2)], own, ls_own).wait()
    for m in range(2):
        for c in range(CHUNKS):
            served[m, pl.ds(pl.multiple_of(z * depth, depth), depth), c * fc : (c + 1) * fc] = (
                own[m, :, c * fc : (c + 1) * fc] * gcol
            ).astype(jnp.bfloat16)

    def arrive_all(d):
        for h in range(HALVES):

            def arrive(s, sign):
                tz(s, 0, h).wait_recv()
                nxt = z - sign

                @pl.when((nxt >= 0) & (nxt < n))
                def _():
                    tz(s, -sign, h).start()

                tx(s, h).start()
                tm(s, t, h).start()

            sides(d, arrive)

    def xrelay(s, sign):
        for h in range(HALVES):
            tx(s, h).wait_recv()
            tm(s, xq, h).start()

    def ycopy(c, p, s):
        ref = strip(g, s, c, p)
        return remote(ref, ref, ss_y, rs_y.at[c], grp=1 - g)

    def yforward(c, p, d):
        def one(s, sign):
            ref = strip(g, s, c, p)
            remote(ref, ref, ss_w, rs_w.at[c, p, s], fs=s).wait_recv()
            ycopy(c, p, s).start()

        sides(d, one)

    def ywait(c):
        ref = wsend.at[:, c]
        remote(ref, ref, ss_y, rs_y.at[c], grp=1 - g).wait_recv()

    def hcopy(c, i, to):
        return remote(hs.at[i, c], hr.at[z, c], ss_h, rs_h.at[c], fs=to)

    def sumsq(s):
        part = jnp.zeros((rows, 128), jnp.float32)
        for q in range(nt):
            for i in range(depth // 128):
                x = tok[s * nt + q, :, i * 128 : (i + 1) * 128].astype(jnp.float32)
                part = part + x * x
        total = jnp.sum(part, axis=-1, keepdims=True)
        scale[s] = jnp.broadcast_to(lax.rsqrt(total / width + 1e-06), (rows, fc))

    def compute(c, i):
        rising = i + jnp.where(i >= z, 1, 0)
        falling = n - 1 - i - jnp.where(n - 1 - i <= z, 1, 0)
        s = jnp.where(i == n - 1, z, jnp.where(2 * z >= n, rising, falling))
        acc = None
        for q in range(nt):
            w = jnp.concatenate(
                [served[m, q * depth : (q + 1) * depth, c * fc : (c + 1) * fc] for m in range(2)], axis=1
            )
            term = jnp.dot(tok[s * nt + q], w, preferred_element_type=jnp.float32)
            acc = term if acc is None else acc + term
        gate = acc[:, :fc] * scale[s]
        up = acc[:, fc:] * scale[s]
        h = (gate / (1.0 + jnp.exp(-gate)) * up).astype(jnp.bfloat16)

        @pl.when(i < n - 1)
        def _():
            hs[i, c] = h
            hcopy(c, i, s).start()

        @pl.when(i == n - 1)
        def _():
            hr[z, c] = h

    arrive_all(1)
    for d in range(2, n - 1):
        arrive_all(d)

    @pl.when(at_end)
    def _():
        for c in range(CHUNKS):
            for p in range(n):
                send_weights(c, p, range(2, n))

    @pl.when(jnp.logical_not(at_end))
    def _():
        for c in range(CHUNKS):
            for p in range(n):
                send_weights(c, p, range(1, n))

    sides(1, xrelay)
    arrive_all(n - 1)
    for p in range(n):
        yforward(0, p, 1)
    for d in range(2, n):
        sides(d, xrelay)
        for p in range(n):
            yforward(0, p, d)

    local(tok_hbm.at[pl.ds(0, rows), pl.ds(0, (nt - 1) * depth)], tok_hbm.at[pl.ds(0, rows), pl.ds(0, (nt - 1) * depth)], ls_tok).wait()
    sumsq(z)

    def rest(s, sign):
        ref = tok.at[pl.ds(0, 2)]
        remote(ref, ref, ss_tok, rs_tm.at[s], tp=mate).wait_recv()
        sumsq(s)

    for d in range(1, n):
        sides(d, rest)
    ywait(0)

    def first(i, carry):
        for d in range(1, n):
            yforward(1, i, d)
        compute(0, i)
        return carry

    lax.fori_loop(0, n, first, 0)
    for copy in small_loads[1:]:
        copy.wait()
    aff = aff_in[...]
    share = aff / jnp.sum(aff, axis=0, keepdims=True)
    top = aff.shape[0]

    def column(row):
        col = jnp.transpose(jnp.broadcast_to(row, (128, rows)))
        return jnp.concatenate([col] * (fc // 128), axis=1) if fc > 128 else col

    shares = [column(share[k : k + 1, :]) for k in range(top)]
    names = [column(names_in[k : k + 1, :].astype(jnp.float32)) for k in range(top)]
    ywait(1)

    def second(i, carry):
        compute(1, i)
        return carry

    lax.fori_loop(0, n, second, 0)

    for c in range(CHUNKS):
        ref = hs.at[:, c]
        remote(ref, ref, ss_h, rs_h.at[c], fs=z).wait_recv()
        picks = []
        for k in range(top):
            picked = jnp.zeros((rows, fc), jnp.float32)
            for e in range(n):
                picked = jnp.where(names[k] == e, hr[e, c].astype(jnp.float32), picked)
            picks.append(picked * shares[k])
        hid_out[:, :, c * fc : (c + 1) * fc] = jnp.stack(picks, axis=1).astype(jnp.bfloat16)

    def sent(ref, sem):
        remote(ref, ref, sem, rs_h.at[0], fs=z).wait_send()

    relayed = 3 * (n - 1)

    @pl.when(at_end)
    def _():
        sent(tok.at[pl.ds(0, relayed + 1)], ss_tok)

    @pl.when(jnp.logical_not(at_end))
    def _():
        sent(tok.at[pl.ds(0, relayed + n + 1)], ss_tok)

    sent(wsend, ss_w)
    sent(wsend, ss_y)
    sent(hs, ss_h)


def emit_kernel(served, hid, gate_out, up_out, hid_out, sems):
    copies = [
        pltpu.make_async_copy(hid, hid_out, sems.at[2]),
        pltpu.make_async_copy(served.at[0], gate_out.at[0], sems.at[0]),
        pltpu.make_async_copy(served.at[1], up_out.at[0], sems.at[1]),
    ]
    for copy in copies:
        copy.start()
    for copy in copies:
        copy.wait()


def dense(tokens, norm_gain, gate_master, up_master, chosen, affinity):
    n, nt = lax.axis_size("fs"), lax.axis_size("tp")
    rows, width = tokens.shape
    experts, depth, fcols = gate_master.shape
    top = chosen.shape[1]
    fc = fcols // CHUNKS
    bf, f32 = jnp.bfloat16, jnp.float32
    dma = pltpu.SemaphoreType.DMA
    hbm = pl.BlockSpec(memory_space=pltpu.HBM)
    vmem = pl.BlockSpec(memory_space=pltpu.VMEM)
    served, hid = pl.pallas_call(
        functools.partial(dense_kernel, n, nt, width),
        out_shape=(
            jax.ShapeDtypeStruct((2, width, fcols), bf),
            jax.ShapeDtypeStruct((rows, top, fcols), bf),
        ),
        in_specs=[hbm] * 6,
        out_specs=(vmem, vmem),
        scratch_shapes=[
            pltpu.VMEM((n * nt, rows, depth), bf),
            pltpu.VMEM((n - 1, depth, fcols), f32),
            pltpu.VMEM((2, depth, fcols), f32),
            pltpu.VMEM((n - 1, CHUNKS, depth, fc), bf),
            pltpu.VMEM((n, rows, fc), f32),
            pltpu.VMEM((n - 1, CHUNKS, rows, fc), bf),
            pltpu.VMEM((n, CHUNKS, rows, fc), bf),
            pltpu.VMEM((1, depth), f32),
            pltpu.VMEM((top, rows), jnp.int32),
            pltpu.VMEM((top, rows), f32),
            dma, dma, dma, dma, dma, dma, dma,
            dma, dma, dma, dma,
            dma((n, HALVES)),
            dma((n, HALVES)),
            dma((n,)),
            dma((CHUNKS, n, n)),
            dma((CHUNKS,)),
            dma((CHUNKS,)),
            pltpu.SemaphoreType.REGULAR((2, n - 2)),
        ],
        compiler_params=pltpu.CompilerParams(
            collective_id=0, has_side_effects=True, vmem_limit_bytes=40 * 1024 * 1024
        ),
    )(*[pltpu.with_memory_space_constraint(x, pltpu.HBM) for x in (tokens, norm_gain.reshape(1, depth), gate_master, up_master, chosen.T, affinity.T)])
    return pl.pallas_call(
        emit_kernel,
        out_shape=(
            jax.ShapeDtypeStruct((1, width, fcols), bf),
            jax.ShapeDtypeStruct((1, width, fcols), bf),
            jax.ShapeDtypeStruct((rows, top, fcols), bf),
        ),
        in_specs=[vmem, vmem],
        out_specs=(hbm, hbm, hbm),
        scratch_shapes=[dma((3,))],
        compiler_params=pltpu.CompilerParams(vmem_limit_bytes=1024 * 1024),
    )(served, hid)


def on_device(tokens, norm_gain, gate_master, up_master, chosen, affinity):
    n, nt = lax.axis_size("fs"), lax.axis_size("tp")
    experts, depth, fcols = gate_master.shape
    rows, width = tokens.shape
    capacity = rows * chosen.shape[1] * 2 // experts
    fits = (
        experts == n
        and capacity >= rows
        and n >= 3
        and nt == 4
        and lax.axis_size("grp") == 2
        and width == nt * depth
        and fcols % (CHUNKS * 128) == 0
        and depth % (16 * n) == 0
    )
    run = dense if fits else routed
    return run(tokens, norm_gain, gate_master, up_master, chosen, affinity)


def solution(mesh):
    return jax.shard_map(
        on_device,
        mesh=mesh,
        in_specs=(
            P(("grp", "fs"), None),
            P("fs"),
            P(None, "fs", "tp"),
            P(None, "fs", "tp"),
            P(("grp", "fs"), None),
            P(("grp", "fs"), None),
        ),
        out_specs=(
            P(("grp", "fs"), None, "tp"),
            P(("grp", "fs"), None, "tp"),
            P(("grp", "fs"), None, "tp"),
        ),
        check_vma=False,
    )
```

time: 61.7 us -> 58.3 us (0.945)
  local copies, waits for them, and re-layouts: 4.74 us -> 0 us
  Pallas kernels: 56.1 us -> 57.5 us
    unnamed x8 -> x0, local copies, waits for them, and re-layouts: 3.98 us -> none
    pallas_call x0 -> x1, Pallas kernels: none -> 1.43 us  [dense(): pl.pallas_call(emit_kernel, out_shape=(jax.ShapeDtypeStruct((1, width, fc...]
    reshape x1 -> x0, local copies, waits for them, and re-layouts: 0.77 us -> none  [dense(): return (gate, up, hid.reshape(rows, top, fcols))]
where the time goes in v1:
time: 58.3 us; the launch traced here: 58.2 us
  Pallas kernels  57.5 us (99%)
  between operations  0.64 us (1%)
    pallas_call x1, Pallas kernels, dense(): pl.pallas_call(functools.partial(dense_kernel, n, nt, width), out_shape=(...  56.1 us
    pallas_call x1, Pallas kernels, dense(): pl.pallas_call(emit_kernel, out_shape=(jax.ShapeDtypeStruct((1, width, fc...  1.43 us

profile of v1, /device:TPU:0, one launch (start us, length us, event | category | flops | bytes accessed | tf_op | source)
XLA Modules:
  0.0 58.2 jit_solution(16321393084977396875)
XLA Ops:
  0.6 56.1 %shard_map.85 = (bf16[2,2048,256]{2,1,0:T(8,128)(2,1)S(1)}, bf16[256,2,256]{2,1,0:T(2,128)(2,1)S(1)}) custom-call(bf16[256,2048]{1,0:T(8,128)(2,1)} %tok_hbm.1, f32[1,512]{1,0:T(1,128)} %bitcast.3, f32[4,512,256]{2,1,0:T(8,128)} %gate_hbm.1, f32[4,512,256]{2,1,0:T(8,128)} %up_hbm.1, s32[2,256]{1,0:T(2,128)} %bitcast.4, f32[2,256]{1,0:T(2,128)} %bitcast.5), custom_call_target="tpu_custom_call" | custom-call | tf_op jit(solution)/shard_map/pallas_call | solution.py:423
  56.7 1.4 %shard_map.86 = (bf16[1,2048,256]{2,1,0:T(8,128)(2,1)}, bf16[1,2048,256]{2,1,0:T(8,128)(2,1)}, bf16[256,2,256]{2,1,0:T(2,128)(2,1)}) custom-call(bf16[2,2048,256]{2,1,0:T(8,128)(2,1)S(1)} %get-tuple-element.5.served, bf16[256,2,256]{2,1,0:T(2,128)(2,1)S(1)} %get-tuple-element.6.hid), custom_call_target="tpu_custom_call" | custom-call | tf_op jit(solution)/shard_map/pallas_call | solution.py:456

commit v2 on v1

--- a/solution.py
+++ b/solution.py
@@ -168,8 +168,9 @@
             def _():
                 fn(s, sign)
 
-    own_load.wait()
-    pl.semaphore_wait(barrier, 5 - jnp.where(at_end, 1, 0))
+    with jax.named_scope('barrier'):
+        own_load.wait()
+        pl.semaphore_wait(barrier, 5 - jnp.where(at_end, 1, 0))
 
     for h in range(HALVES):
         sides(1, lambda s, sign: tz(z, sign, h).start())
@@ -182,10 +183,12 @@
     def slot(s):
         return lax.rem(s - z + n, n) - 1
 
-    small_loads[0].wait()
+    with jax.named_scope('gain'):
+        small_loads[0].wait()
     gcol = jnp.transpose(jnp.broadcast_to(gain[...], (128, depth)))
     gcol = jnp.concatenate([gcol] * (fc // 128), axis=1) if fc > 128 else gcol
-    local(gate_hbm.at[pl.ds(0, n - 1)], wf, ls_w).wait()
+    with jax.named_scope('wload'):
+        local(gate_hbm.at[pl.ds(0, n - 1)], wf, ls_w).wait()
     for k in range(n - 1):
         for c in range(CHUNKS):
             wsend[k, c] = (wf[k, :, c * fc : (c + 1) * fc] * gcol).astype(jnp.bfloat16)
@@ -200,10 +203,6 @@
                 def _():
                     signal(far.at[way, k + 1], fs=z + step)
 
-    for k in range(n - 2):
-        hears(k, n - 2 - z, 0, has_dn, -1)
-        hears(k, z - 1, 1, has_up, 1)
-
     def part(s, p):
         size = depth // n
         return pl.ds(pl.multiple_of(s * depth + p * size, size), size)
@@ -215,15 +214,18 @@
         src = wsend.at[slot(to), c, part(0, p)]
         return remote(src, strip(g, z, c, p), ss_w, rs_w.at[c, p, z], fs=to)
 
-    def send_weights(c, p, distances):
-        for d in distances:
-            sides(d, lambda s, sign: wcopy(c, p, s).start())
-
-    @pl.when(at_end)
-    def _():
-        for c in range(CHUNKS):
-            for p in range(n):
-                send_weights(c, p, (1,))
+    def send_weights(c, d, sign):
+        for p in range(n):
+            wcopy(c, p, z + sign * d).start()
+
+    for c in range(CHUNKS):
+        for there, sign in ((has_up, 1), (has_dn, -1)):
+            pl.when(there)(functools.partial(send_weights, c, 1, sign))
+
+    with jax.named_scope('hears'):
+        for k in range(n - 2):
+            hears(k, n - 2 - z, 0, has_dn, -1)
+            hears(k, z - 1, 1, has_up, 1)
 
     local(gate_hbm.at[pl.ds(0, 2)], own, ls_own).wait()
     for m in range(2):
@@ -257,13 +259,18 @@
         ref = strip(g, s, c, p)
         return remote(ref, ref, ss_y, rs_y.at[c], grp=1 - g)
 
-    def yforward(c, p, d):
+    def yforward(c, d, side=None):
         def one(s, sign):
-            ref = strip(g, s, c, p)
-            remote(ref, ref, ss_w, rs_w.at[c, p, s], fs=s).wait_recv()
-            ycopy(c, p, s).start()
-
-        sides(d, one)
+            for p in range(n):
+                ref = strip(g, s, c, p)
+                remote(ref, ref, ss_w, rs_w.at[c, p, s], fs=s).wait_recv()
+                ycopy(c, p, s).start()
+
+        def one_side(s, sign):
+            outer = (s == 0) | (s == n - 1)
+            pl.when(outer if side == "outer" else jnp.logical_not(outer))(lambda: one(s, sign))
+
+        sides(d, one_side if side else one)
 
     def ywait(c):
         ref = wsend.at[:, c]
@@ -285,10 +292,11 @@
         rising = i + jnp.where(i >= z, 1, 0)
         falling = n - 1 - i - jnp.where(n - 1 - i <= z, 1, 0)
         s = jnp.where(i == n - 1, z, jnp.where(2 * z >= n, rising, falling))
+        strips = pl.ds(pl.multiple_of(c * fc, fc), fc)
         acc = None
         for q in range(nt):
             w = jnp.concatenate(
-                [served[m, q * depth : (q + 1) * depth, c * fc : (c + 1) * fc] for m in range(2)], axis=1
+                [served[m, q * depth : (q + 1) * depth, strips] for m in range(2)], axis=1
             )
             term = jnp.dot(tok[s * nt + q], w, preferred_element_type=jnp.float32)
             acc = term if acc is None else acc + term
@@ -305,32 +313,22 @@
         def _():
             hr[z, c] = h
 
-    arrive_all(1)
-    for d in range(2, n - 1):
-        arrive_all(d)
-
-    @pl.when(at_end)
-    def _():
-        for c in range(CHUNKS):
-            for p in range(n):
-                send_weights(c, p, range(2, n))
-
-    @pl.when(jnp.logical_not(at_end))
-    def _():
-        for c in range(CHUNKS):
-            for p in range(n):
-                send_weights(c, p, range(1, n))
-
-    sides(1, xrelay)
-    arrive_all(n - 1)
-    for p in range(n):
-        yforward(0, p, 1)
-    for d in range(2, n):
-        sides(d, xrelay)
-        for p in range(n):
-            yforward(0, p, d)
-
-    local(tok_hbm.at[pl.ds(0, rows), pl.ds(0, (nt - 1) * depth)], tok_hbm.at[pl.ds(0, rows), pl.ds(0, (nt - 1) * depth)], ls_tok).wait()
+    inner = jnp.logical_not(at_end)
+    late = lax.rem(t, 2) == 1
+
+    def send_far():
+        for d in range(2, n):
+            for c in range(CHUNKS):
+                for sign in (1, -1):
+                    s = z + sign * d
+                    pl.when((s >= 0) & (s < n))(functools.partial(send_weights, c, d, sign))
+
+    with jax.named_scope("arr1"):
+        arrive_all(1)
+
+    local(
+        tok_hbm.at[:, pl.ds(0, (nt - 1) * depth)], tok_hbm.at[:, pl.ds(0, (nt - 1) * depth)], ls_tok
+    ).wait()
     sumsq(z)
 
     def rest(s, sign):
@@ -338,17 +336,62 @@
         remote(ref, ref, ss_tok, rs_tm.at[s], tp=mate).wait_recv()
         sumsq(s)
 
-    for d in range(1, n):
-        sides(d, rest)
-    ywait(0)
-
-    def first(i, carry):
-        for d in range(1, n):
-            yforward(1, i, d)
-        compute(0, i)
-        return carry
-
-    lax.fori_loop(0, n, first, 0)
+    def totals():
+        with jax.named_scope("rest"):
+            for d in range(1, n):
+                sides(d, rest)
+
+    @pl.when(at_end)
+    def _():
+        with jax.named_scope("yf0_1"):
+            yforward(0, 1)
+        with jax.named_scope("xr1"):
+            sides(1, xrelay)
+        with jax.named_scope("yf1_1"):
+            yforward(1, 1)
+        for d in range(2, n - 1):
+            with jax.named_scope("arr2"):
+                arrive_all(d)
+        send_far()
+        for d in range(2, n - 1):
+            with jax.named_scope("xr2"):
+                sides(d, xrelay)
+        with jax.named_scope("arr3"):
+            arrive_all(n - 1)
+        with jax.named_scope("yf0_3"):
+            yforward(0, n - 1)
+        with jax.named_scope("xr3"):
+            sides(n - 1, xrelay)
+        with jax.named_scope("yf1_3"):
+            yforward(1, n - 1)
+        totals()
+        for c in range(CHUNKS):
+            for d in range(2, n - 1):
+                with jax.named_scope("yf%d_2" % c):
+                    yforward(c, d)
+
+    @pl.when(inner)
+    def _():
+        for c in range(CHUNKS):
+            with jax.named_scope("yf%d_1" % c):
+                yforward(c, 1)
+        with jax.named_scope("xr1"):
+            sides(1, xrelay)
+        for d in range(2, n - 1):
+            with jax.named_scope("arr2"):
+                arrive_all(d)
+        for d in range(2, n - 1):
+            with jax.named_scope("yf0_2"):
+                yforward(0, d)
+        send_far()
+        for d in range(2, n - 1):
+            with jax.named_scope("xr2"):
+                sides(d, xrelay)
+        for d in range(2, n - 1):
+            with jax.named_scope("yf1_2"):
+                yforward(1, d)
+        totals()
+
     for copy in small_loads[1:]:
         copy.wait()
     aff = aff_in[...]
@@ -361,17 +404,27 @@
 
     shares = [column(share[k : k + 1, :]) for k in range(top)]
     names = [column(names_in[k : k + 1, :].astype(jnp.float32)) for k in range(top)]
-    ywait(1)
-
-    def second(i, carry):
-        compute(1, i)
+    with jax.named_scope("yw0"):
+        ywait(0)
+
+    def step(j, carry):
+        @pl.when(j == jnp.where(at_end, n, 0))
+        def _():
+            with jax.named_scope("yw1"):
+                ywait(1)
+
+        c = jnp.where(at_end, j // n, lax.rem(j, CHUNKS))
+        i = jnp.where(at_end, lax.rem(j, n), j // CHUNKS)
+        with jax.named_scope("comp"):
+            compute(c, i)
         return carry
 
-    lax.fori_loop(0, n, second, 0)
+    lax.fori_loop(0, n * CHUNKS, step, 0)
 
     for c in range(CHUNKS):
         ref = hs.at[:, c]
-        remote(ref, ref, ss_h, rs_h.at[c], fs=z).wait_recv()
+        with jax.named_scope('hw%d' % c):
+            remote(ref, ref, ss_h, rs_h.at[c], fs=z).wait_recv()
         picks = []
         for k in range(top):
             picked = jnp.zeros((rows, fc), jnp.float32)
@@ -381,6 +434,7 @@
         hid_out[:, :, c * fc : (c + 1) * fc] = jnp.stack(picks, axis=1).astype(jnp.bfloat16)
 
     def sent(ref, sem):
+      with jax.named_scope('sent'):
         remote(ref, ref, sem, rs_h.at[0], fs=z).wait_send()
 
     relayed = 3 * (n - 1)

time: 58.3 us -> 55.1 us (0.945)
  Pallas kernels: 57.5 us -> 54.3 us
    pallas_call x1, Pallas kernels: 56.1 us -> 52.9 us  [dense(): pl.pallas_call(functools.partial(dense_kernel, n, nt, width), out_shape=(...]
where the time goes in v2:
time: 55.1 us; the launch traced here: 55 us
  Pallas kernels  54.3 us (99%)
  between operations  0.64 us (1%)
    pallas_call x1, Pallas kernels, dense(): pl.pallas_call(functools.partial(dense_kernel, n, nt, width), out_shape=(...  52.9 us
    pallas_call x1, Pallas kernels, dense(): pl.pallas_call(emit_kernel, out_shape=(jax.ShapeDtypeStruct((1, width, fc...  1.43 us

profile of v2, /device:TPU:0, one launch (start us, length us, event | category | flops | bytes accessed | tf_op | source)
XLA Modules:
  0.0 55.0 jit_solution(2164605409747502216)
XLA Ops:
  0.6 52.9 %shard_map.85 = (bf16[2,2048,256]{2,1,0:T(8,128)(2,1)S(1)}, bf16[256,2,256]{2,1,0:T(2,128)(2,1)S(1)}) custom-call(bf16[256,2048]{1,0:T(8,128)(2,1)} %tok_hbm.1, f32[1,512]{1,0:T(1,128)} %bitcast.3, f32[4,512,256]{2,1,0:T(8,128)} %gate_hbm.1, f32[4,512,256]{2,1,0:T(8,128)} %up_hbm.1, s32[2,256]{1,0:T(2,128)} %bitcast.4, f32[2,256]{1,0:T(2,128)} %bitcast.5), custom_call_target="tpu_custom_call" | custom-call | tf_op jit(solution)/shard_map/pallas_call | solution.py:477
  53.6 1.4 %shard_map.86 = (bf16[1,2048,256]{2,1,0:T(8,128)(2,1)}, bf16[1,2048,256]{2,1,0:T(8,128)(2,1)}, bf16[256,2,256]{2,1,0:T(2,128)(2,1)}) custom-call(bf16[2,2048,256]{2,1,0:T(8,128)(2,1)S(1)} %get-tuple-element.5.served, bf16[256,2,256]{2,1,0:T(2,128)(2,1)S(1)} %get-tuple-element.6.hid), custom_call_target="tpu_custom_call" | custom-call | tf_op jit(solution)/shard_map/pallas_call | solution.py:510

commit v3 on v2

--- a/solution.py
+++ b/solution.py
@@ -408,13 +408,14 @@
         ywait(0)
 
     def step(j, carry):
-        @pl.when(j == jnp.where(at_end, n, 0))
+        @pl.when(j == jnp.where(at_end, n - 2, 0))
         def _():
             with jax.named_scope("yw1"):
                 ywait(1)
 
-        c = jnp.where(at_end, j // n, lax.rem(j, CHUNKS))
-        i = jnp.where(at_end, lax.rem(j, n), j // CHUNKS)
+        split = at_end & (j < CHUNKS * (n - 2))
+        c = jnp.where(split, j // (n - 2), lax.rem(j, CHUNKS))
+        i = jnp.where(split, lax.rem(j, n - 2), j // CHUNKS)
         with jax.named_scope("comp"):
             compute(c, i)
         return carry

time: 55.1 us -> 54.1 us (0.982)
  Pallas kernels: 54.3 us -> 53.3 us
    pallas_call x1, Pallas kernels: 52.9 us -> 51.9 us  [dense(): pl.pallas_call(functools.partial(dense_kernel, n, nt, width), out_shape=(...]
where the time goes in v3:
time: 54.1 us; the launch traced here: 54 us
  Pallas kernels  53.3 us (99%)
  between operations  0.64 us (1%)
    pallas_call x1, Pallas kernels, dense(): pl.pallas_call(functools.partial(dense_kernel, n, nt, width), out_shape=(...  51.9 us
    pallas_call x1, Pallas kernels, dense(): pl.pallas_call(emit_kernel, out_shape=(jax.ShapeDtypeStruct((1, width, fc...  1.43 us

profile of v3, /device:TPU:0, one launch (start us, length us, event | category | flops | bytes accessed | tf_op | source)
XLA Modules:
  0.0 54.0 jit_solution(8197611026208566530)
XLA Ops:
  0.6 51.9 %shard_map.85 = (bf16[2,2048,256]{2,1,0:T(8,128)(2,1)S(1)}, bf16[256,2,256]{2,1,0:T(2,128)(2,1)S(1)}) custom-call(bf16[256,2048]{1,0:T(8,128)(2,1)} %tok_hbm.1, f32[1,512]{1,0:T(1,128)} %bitcast.3, f32[4,512,256]{2,1,0:T(8,128)} %gate_hbm.1, f32[4,512,256]{2,1,0:T(8,128)} %up_hbm.1, s32[2,256]{1,0:T(2,128)} %bitcast.4, f32[2,256]{1,0:T(2,128)} %bitcast.5), custom_call_target="tpu_custom_call" | custom-call | tf_op jit(solution)/shard_map/pallas_call | solution.py:478
  52.6 1.4 %shard_map.86 = (bf16[1,2048,256]{2,1,0:T(8,128)(2,1)}, bf16[1,2048,256]{2,1,0:T(8,128)(2,1)}, bf16[256,2,256]{2,1,0:T(2,128)(2,1)}) custom-call(bf16[2,2048,256]{2,1,0:T(8,128)(2,1)S(1)} %get-tuple-element.5.served, bf16[256,2,256]{2,1,0:T(2,128)(2,1)S(1)} %get-tuple-element.6.hid), custom_call_target="tpu_custom_call" | custom-call | tf_op jit(solution)/shard_map/pallas_call | solution.py:511

commit v4 on v2

--- a/solution.py
+++ b/solution.py
@@ -76,8 +76,8 @@
 def dense_kernel(
     n, nt, width,
     tok_hbm, gain_hbm, gate_hbm, up_hbm, chosen_hbm, aff_hbm,
-    served, hid_out,
-    tok, wf, own, wsend, scale, hs, hr, gain, names_in, aff_in,
+    served, hr, names, shares,
+    tok, wf, own, wsend, scale, hs, gain, names_in, aff_in,
     ls_own_tok, ls_tok, ls_w, ls_own, ls_gain, ls_names, ls_aff,
     ss_tok, ss_w, ss_y, ss_h, rs_tz, rs_tx, rs_tm, rs_w, rs_y, rs_h, far,
 ):
@@ -101,6 +101,9 @@
     def signal(sem, **dev):
         pl.semaphore_signal(sem, 1, device_id=dev, device_id_type=MESH)
 
+    def slot(s):
+        return lax.rem(s - z + 2 * n, n) - 1
+
     barrier = pltpu.get_barrier_semaphore()
     for there, step in ((has_up, 1), (has_dn, -1)):
 
@@ -150,15 +153,15 @@
 
     def tz(s, step, h):
         ref = block(s, t, h)
-        return remote(ref, ref, ss_tok, rs_tz.at[s, h], fs=z + step)
+        return remote(ref, ref, ss_tok, rs_tz.at[slot(s - step), h], fs=z + step)
 
     def tx(s, h):
         ref = block(s, t, h)
-        return remote(ref, ref, ss_tok, rs_tx.at[s, h], tp=xq)
+        return remote(ref, ref, ss_tok, rs_tx.at[slot(s), h], tp=xq)
 
     def tm(s, q, h):
         ref = block(s, q, h)
-        return remote(ref, ref, ss_tok, rs_tm.at[s], tp=mate)
+        return remote(ref, ref, ss_tok, rs_tm.at[slot(s)], tp=mate)
 
     def sides(d, fn):
         for sign in (1, -1):
@@ -168,8 +171,9 @@
             def _():
                 fn(s, sign)
 
+    with jax.named_scope('tokload'):
+        own_load.wait()
     with jax.named_scope('barrier'):
-        own_load.wait()
         pl.semaphore_wait(barrier, 5 - jnp.where(at_end, 1, 0))
 
     for h in range(HALVES):
@@ -179,9 +183,6 @@
     def _():
         signal(far.at[0, 0], fs=z - 1)
         signal(far.at[1, 0], fs=z + 1)
-
-    def slot(s):
-        return lax.rem(s - z + n, n) - 1
 
     with jax.named_scope('gain'):
         small_loads[0].wait()
@@ -212,7 +213,7 @@
 
     def wcopy(c, p, to):
         src = wsend.at[slot(to), c, part(0, p)]
-        return remote(src, strip(g, z, c, p), ss_w, rs_w.at[c, p, z], fs=to)
+        return remote(src, strip(g, z, c, p), ss_w, rs_w.at[c, p, lax.rem(z - to + n, n) - 1], fs=to)
 
     def send_weights(c, d, sign):
         for p in range(n):
@@ -220,7 +221,14 @@
 
     for c in range(CHUNKS):
         for there, sign in ((has_up, 1), (has_dn, -1)):
-            pl.when(there)(functools.partial(send_weights, c, 1, sign))
+            outward = at_end | (z + sign == 0) | (z + sign == n - 1)
+            now = there if c == 0 else there & outward
+            pl.when(now)(functools.partial(send_weights, c, 1, sign))
+
+    def send_to(c, d):
+        for sign in (1, -1):
+            s = z + sign * d
+            pl.when((s >= 0) & (s < n))(functools.partial(send_weights, c, d, sign))
 
     with jax.named_scope('hears'):
         for k in range(n - 2):
@@ -234,21 +242,25 @@
                 own[m, :, c * fc : (c + 1) * fc] * gcol
             ).astype(jnp.bfloat16)
 
-    def arrive_all(d):
+    def arrive_half(d, h):
+        def arrive(s, sign):
+            tz(s, 0, h).wait_recv()
+            nxt = z - sign
+
+            @pl.when((nxt >= 0) & (nxt < n))
+            def _():
+                tz(s, -sign, h).start()
+
+            tx(s, h).start()
+            tm(s, t, h).start()
+
+        sides(d, arrive)
+
+    def arrive_all(d, between=None):
         for h in range(HALVES):
-
-            def arrive(s, sign):
-                tz(s, 0, h).wait_recv()
-                nxt = z - sign
-
-                @pl.when((nxt >= 0) & (nxt < n))
-                def _():
-                    tz(s, -sign, h).start()
-
-                tx(s, h).start()
-                tm(s, t, h).start()
-
-            sides(d, arrive)
+            if between and h == HALVES - 1:
+                between()
+            arrive_half(d, h)
 
     def xrelay(s, sign):
         for h in range(HALVES):
@@ -259,11 +271,11 @@
         ref = strip(g, s, c, p)
         return remote(ref, ref, ss_y, rs_y.at[c], grp=1 - g)
 
-    def yforward(c, d, side=None):
+    def yforward(c, d, side=None, piece=None):
         def one(s, sign):
-            for p in range(n):
+            for p in range(n) if piece is None else (piece,):
                 ref = strip(g, s, c, p)
-                remote(ref, ref, ss_w, rs_w.at[c, p, s], fs=s).wait_recv()
+                remote(ref, ref, ss_w, rs_w.at[c, p, slot(s)], fs=s).wait_recv()
                 ycopy(c, p, s).start()
 
         def one_side(s, sign):
@@ -277,7 +289,7 @@
         remote(ref, ref, ss_y, rs_y.at[c], grp=1 - g).wait_recv()
 
     def hcopy(c, i, to):
-        return remote(hs.at[i, c], hr.at[z, c], ss_h, rs_h.at[c], fs=to)
+        return remote(hs.at[i, c], hr.at[z, c], ss_h, rs_h, fs=to)
 
     def sumsq(s):
         part = jnp.zeros((rows, 128), jnp.float32)
@@ -316,15 +328,30 @@
     inner = jnp.logical_not(at_end)
     late = lax.rem(t, 2) == 1
 
+    slow = lax.rem(t, 2) == 0
+
     def send_far():
         for d in range(2, n):
             for c in range(CHUNKS):
-                for sign in (1, -1):
-                    s = z + sign * d
-                    pl.when((s >= 0) & (s < n))(functools.partial(send_weights, c, d, sign))
+                send_to(c, d)
+
+    def send_mid():
+        for d in range(2, n):
+            send_to(0, d)
+        for sign in (1, -1):
+            s = z + sign
+            here = (s > 0) & (s < n - 1)
+            for c in range(1, CHUNKS):
+                pl.when(here)(functools.partial(send_weights, c, 1, sign))
+
+    def send_last():
+        for c in range(1, CHUNKS):
+            for d in range(2, n):
+                send_to(c, d)
 
     with jax.named_scope("arr1"):
         arrive_all(1)
+    pl.when(inner)(send_mid)
 
     local(
         tok_hbm.at[:, pl.ds(0, (nt - 1) * depth)], tok_hbm.at[:, pl.ds(0, (nt - 1) * depth)], ls_tok
@@ -333,7 +360,7 @@
 
     def rest(s, sign):
         ref = tok.at[pl.ds(0, 2)]
-        remote(ref, ref, ss_tok, rs_tm.at[s], tp=mate).wait_recv()
+        remote(ref, ref, ss_tok, rs_tm.at[slot(s)], tp=mate).wait_recv()
         sumsq(s)
 
     def totals():
@@ -351,13 +378,19 @@
             yforward(1, 1)
         for d in range(2, n - 1):
             with jax.named_scope("arr2"):
-                arrive_all(d)
-        send_far()
+                arrive_all(d, (lambda: pl.when(slow)(send_far)) if d == n - 2 else None)
+        pl.when(jnp.logical_not(slow))(send_far)
         for d in range(2, n - 1):
             with jax.named_scope("xr2"):
                 sides(d, xrelay)
-        with jax.named_scope("arr3"):
-            arrive_all(n - 1)
+        for d in range(2, n - 1):
+            with jax.named_scope("yf0_2"):
+                yforward(0, d)
+        with jax.named_scope("arr3a"):
+            arrive_half(n - 1, 0)
+        for h in range(1, HALVES):
+            with jax.named_scope("arr3b"):
+                arrive_half(n - 1, h)
         with jax.named_scope("yf0_3"):
             yforward(0, n - 1)
         with jax.named_scope("xr3"):
@@ -365,16 +398,13 @@
         with jax.named_scope("yf1_3"):
             yforward(1, n - 1)
         totals()
-        for c in range(CHUNKS):
-            for d in range(2, n - 1):
-                with jax.named_scope("yf%d_2" % c):
-                    yforward(c, d)
 
     @pl.when(inner)
     def _():
-        for c in range(CHUNKS):
-            with jax.named_scope("yf%d_1" % c):
-                yforward(c, 1)
+        with jax.named_scope("yf0_1"):
+            yforward(0, 1)
+        with jax.named_scope("yf1_o"):
+            yforward(1, 1, "outer")
         with jax.named_scope("xr1"):
             sides(1, xrelay)
         for d in range(2, n - 1):
@@ -383,7 +413,7 @@
         for d in range(2, n - 1):
             with jax.named_scope("yf0_2"):
                 yforward(0, d)
-        send_far()
+        send_last()
         for d in range(2, n - 1):
             with jax.named_scope("xr2"):
                 sides(d, xrelay)
@@ -391,51 +421,52 @@
             with jax.named_scope("yf1_2"):
                 yforward(1, d)
         totals()
+        with jax.named_scope("yf1_i"):
+            yforward(1, 1, "inner")
 
     for copy in small_loads[1:]:
         copy.wait()
     aff = aff_in[...]
     share = aff / jnp.sum(aff, axis=0, keepdims=True)
-    top = aff.shape[0]
 
     def column(row):
         col = jnp.transpose(jnp.broadcast_to(row, (128, rows)))
         return jnp.concatenate([col] * (fc // 128), axis=1) if fc > 128 else col
 
-    shares = [column(share[k : k + 1, :]) for k in range(top)]
-    names = [column(names_in[k : k + 1, :].astype(jnp.float32)) for k in range(top)]
+    for k in range(aff.shape[0]):
+        shares[k] = column(share[k : k + 1, :])
+        names[k] = column(names_in[k : k + 1, :].astype(jnp.float32))
     with jax.named_scope("yw0"):
         ywait(0)
 
     def step(j, carry):
-        @pl.when(j == jnp.where(at_end, n, 0))
+        with jax.named_scope("yf1_2"):
+
+            @pl.when(at_end & (j < n))
+            def _():
+                for d in range(2, n - 1):
+                    yforward(1, d, piece=j)
+
+        @pl.when(j == n - 1)
         def _():
             with jax.named_scope("yw1"):
                 ywait(1)
 
-        c = jnp.where(at_end, j // n, lax.rem(j, CHUNKS))
-        i = jnp.where(at_end, lax.rem(j, n), j // CHUNKS)
+        split = j < CHUNKS * (n - 1)
+        c = jnp.where(split, j // (n - 1), lax.rem(j, CHUNKS))
+        i = jnp.where(split, lax.rem(j, n - 1), j // CHUNKS)
         with jax.named_scope("comp"):
             compute(c, i)
         return carry
 
     lax.fori_loop(0, n * CHUNKS, step, 0)
 
-    for c in range(CHUNKS):
-        ref = hs.at[:, c]
-        with jax.named_scope('hw%d' % c):
-            remote(ref, ref, ss_h, rs_h.at[c], fs=z).wait_recv()
-        picks = []
-        for k in range(top):
-            picked = jnp.zeros((rows, fc), jnp.float32)
-            for e in range(n):
-                picked = jnp.where(names[k] == e, hr[e, c].astype(jnp.float32), picked)
-            picks.append(picked * shares[k])
-        hid_out[:, :, c * fc : (c + 1) * fc] = jnp.stack(picks, axis=1).astype(jnp.bfloat16)
+    with jax.named_scope("hw"):
+        remote(hs, hs, ss_h, rs_h, fs=z).wait_recv()
 
     def sent(ref, sem):
       with jax.named_scope('sent'):
-        remote(ref, ref, sem, rs_h.at[0], fs=z).wait_send()
+        remote(ref, ref, sem, rs_h, fs=z).wait_send()
 
     relayed = 3 * (n - 1)
 
@@ -452,14 +483,26 @@
     sent(hs, ss_h)
 
 
-def emit_kernel(served, hid, gate_out, up_out, hid_out, sems):
+def emit_kernel(served, hr, names, shares, gate_out, up_out, hid_out, hid, sems):
+    n, chunks, rows, fc = hr.shape
     copies = [
-        pltpu.make_async_copy(hid, hid_out, sems.at[2]),
         pltpu.make_async_copy(served.at[0], gate_out.at[0], sems.at[0]),
         pltpu.make_async_copy(served.at[1], up_out.at[0], sems.at[1]),
     ]
     for copy in copies:
         copy.start()
+    for c in range(chunks):
+        picks = []
+        for k in range(names.shape[0]):
+            picked = jnp.zeros((rows, fc), jnp.float32)
+            for e in range(n):
+                picked = jnp.where(names[k] == e, hr[e, c].astype(jnp.float32), picked)
+            picks.append(picked * shares[k])
+        hid[c] = jnp.stack(picks, axis=1).astype(jnp.bfloat16)
+        copies.append(
+            pltpu.make_async_copy(hid.at[c], hid_out.at[:, :, pl.ds(c * fc, fc)], sems.at[2 + c])
+        )
+        copies[-1].start()
     for copy in copies:
         copy.wait()
 
@@ -474,14 +517,16 @@
     dma = pltpu.SemaphoreType.DMA
     hbm = pl.BlockSpec(memory_space=pltpu.HBM)
     vmem = pl.BlockSpec(memory_space=pltpu.VMEM)
-    served, hid = pl.pallas_call(
+    parts = pl.pallas_call(
         functools.partial(dense_kernel, n, nt, width),
         out_shape=(
             jax.ShapeDtypeStruct((2, width, fcols), bf),
-            jax.ShapeDtypeStruct((rows, top, fcols), bf),
+            jax.ShapeDtypeStruct((n, CHUNKS, rows, fc), bf),
+            jax.ShapeDtypeStruct((top, rows, fc), f32),
+            jax.ShapeDtypeStruct((top, rows, fc), f32),
         ),
         in_specs=[hbm] * 6,
-        out_specs=(vmem, vmem),
+        out_specs=(vmem,) * 4,
         scratch_shapes=[
             pltpu.VMEM((n * nt, rows, depth), bf),
             pltpu.VMEM((n - 1, depth, fcols), f32),
@@ -489,18 +534,17 @@
             pltpu.VMEM((n - 1, CHUNKS, depth, fc), bf),
             pltpu.VMEM((n, rows, fc), f32),
             pltpu.VMEM((n - 1, CHUNKS, rows, fc), bf),
-            pltpu.VMEM((n, CHUNKS, rows, fc), bf),
             pltpu.VMEM((1, depth), f32),
             pltpu.VMEM((top, rows), jnp.int32),
             pltpu.VMEM((top, rows), f32),
             dma, dma, dma, dma, dma, dma, dma,
             dma, dma, dma, dma,
-            dma((n, HALVES)),
-            dma((n, HALVES)),
-            dma((n,)),
-            dma((CHUNKS, n, n)),
+            dma((n - 1, HALVES)),
+            dma((n - 1, HALVES)),
+            dma((n - 1,)),
+            dma((CHUNKS, n, n - 1)),
             dma((CHUNKS,)),
-            dma((CHUNKS,)),
+            dma,
             pltpu.SemaphoreType.REGULAR((2, n - 2)),
         ],
         compiler_params=pltpu.CompilerParams(
@@ -514,11 +558,11 @@
             jax.ShapeDtypeStruct((1, width, fcols), bf),
             jax.ShapeDtypeStruct((rows, top, fcols), bf),
         ),
-        in_specs=[vmem, vmem],
+        in_specs=[vmem] * 4,
         out_specs=(hbm, hbm, hbm),
-        scratch_shapes=[dma((3,))],
+        scratch_shapes=[pltpu.VMEM((CHUNKS, rows, top, fc), bf), dma((2 + CHUNKS,))],
         compiler_params=pltpu.CompilerParams(vmem_limit_bytes=1024 * 1024),
-    )(served, hid)
+    )(*parts)
 
 
 def on_device(tokens, norm_gain, gate_master, up_master, chosen, affinity):

time: 55.1 us -> 53.7 us (0.975)
  Pallas kernels: 54.3 us -> 52.9 us
    pallas_call x1, Pallas kernels: 52.9 us -> 51.4 us  [dense(): pl.pallas_call(functools.partial(dense_kernel, n, nt, width), out_shape=(...]
where the time goes in v4:
time: 53.7 us; the launch traced here: 53.5 us
  Pallas kernels  52.9 us (99%)
  between operations  0.64 us (1%)
    pallas_call x1, Pallas kernels, dense(): pl.pallas_call(functools.partial(dense_kernel, n, nt, width), out_shape=(...  51.4 us
    pallas_call x1, Pallas kernels, dense(): pl.pallas_call(emit_kernel, out_shape=(jax.ShapeDtypeStruct((1, width, fc...  1.43 us

profile of v4, /device:TPU:0, one launch (start us, length us, event | category | flops | bytes accessed | tf_op | source)
XLA Modules:
  0.0 53.5 jit_solution(11407749472155465135)
XLA Ops:
  0.6 51.4 %shard_map.85 = (bf16[2,2048,256]{2,1,0:T(8,128)(2,1)S(1)}, bf16[4,2,256,128]{3,2,1,0:T(8,128)(2,1)S(1)}, f32[2,256,128]{2,1,0:T(8,128)S(1)}, f32[2,256,128]{2,1,0:T(8,128)S(1)}) custom-call(bf16[256,2048]{1,0:T(8,128)(2,1)} %tok_hbm.1, f32[1,512]{1,0:T(1,128)} %bitcast.3, f32[4,512,256]{2,1,0:T(8,128)} %gate_hbm.1, f32[4,512,256]{2,1,0:T(8,128)} %up_hbm.1, ...), custom_call_target="tpu_custom_call" | custom-call | tf_op jit(solution)/shard_map/pallas_call | solution.py:520
  52.1 1.4 %shard_map.86 = (bf16[1,2048,256]{2,1,0:T(8,128)(2,1)}, bf16[1,2048,256]{2,1,0:T(8,128)(2,1)}, bf16[256,2,256]{2,1,0:T(2,128)(2,1)}) custom-call(bf16[2,2048,256]{2,1,0:T(8,128)(2,1)S(1)} %get-tuple-element.7.served, bf16[4,2,256,128]{3,2,1,0:T(8,128)(2,1)S(1)} %get-tuple-element.8.hr, f32[2,256,128]{2,1,0:T(8,128)S(1)} %get-tuple-element.9.names, ...), custom_call_target="tpu_custom_call" | custom-call | tf_op jit(solution)/shard_map/pallas_call | solution.py:554

commit v5 on v4

--- a/solution.py
+++ b/solution.py
@@ -215,8 +215,8 @@
         src = wsend.at[slot(to), c, part(0, p)]
         return remote(src, strip(g, z, c, p), ss_w, rs_w.at[c, p, lax.rem(z - to + n, n) - 1], fs=to)
 
-    def send_weights(c, d, sign):
-        for p in range(n):
+    def send_weights(c, d, sign, pieces=None):
+        for p in pieces or range(n):
             wcopy(c, p, z + sign * d).start()
 
     for c in range(CHUNKS):
@@ -225,10 +225,10 @@
             now = there if c == 0 else there & outward
             pl.when(now)(functools.partial(send_weights, c, 1, sign))
 
-    def send_to(c, d):
+    def send_to(c, d, pieces=None):
         for sign in (1, -1):
             s = z + sign * d
-            pl.when((s >= 0) & (s < n))(functools.partial(send_weights, c, d, sign))
+            pl.when((s >= 0) & (s < n))(functools.partial(send_weights, c, d, sign, pieces))
 
     with jax.named_scope('hears'):
         for k in range(n - 2):
@@ -300,10 +300,13 @@
         total = jnp.sum(part, axis=-1, keepdims=True)
         scale[s] = jnp.broadcast_to(lax.rsqrt(total / width + 1e-06), (rows, fc))
 
-    def compute(c, i):
+    def target(i):
         rising = i + jnp.where(i >= z, 1, 0)
         falling = n - 1 - i - jnp.where(n - 1 - i <= z, 1, 0)
-        s = jnp.where(i == n - 1, z, jnp.where(2 * z >= n, rising, falling))
+        return jnp.where(i == n - 1, z, jnp.where(2 * z >= n, rising, falling))
+
+    def compute(c, i, held):
+        s = target(i)
         strips = pl.ds(pl.multiple_of(c * fc, fc), fc)
         acc = None
         for q in range(nt):
@@ -319,7 +322,7 @@
         @pl.when(i < n - 1)
         def _():
             hs[i, c] = h
-            hcopy(c, i, s).start()
+            pl.when(jnp.logical_not(held))(lambda: hcopy(c, i, s).start())
 
         @pl.when(i == n - 1)
         def _():
@@ -344,14 +347,17 @@
             for c in range(1, CHUNKS):
                 pl.when(here)(functools.partial(send_weights, c, 1, sign))
 
-    def send_last():
+    soon = z == n - 2
+
+    def send_last(pieces):
         for c in range(1, CHUNKS):
             for d in range(2, n):
-                send_to(c, d)
+                send_to(c, d, pieces)
 
     with jax.named_scope("arr1"):
         arrive_all(1)
     pl.when(inner)(send_mid)
+    pl.when(inner & soon)(lambda: send_last(range(1)))
 
     local(
         tok_hbm.at[:, pl.ds(0, (nt - 1) * depth)], tok_hbm.at[:, pl.ds(0, (nt - 1) * depth)], ls_tok
@@ -413,7 +419,8 @@
         for d in range(2, n - 1):
             with jax.named_scope("yf0_2"):
                 yforward(0, d)
-        send_last()
+        send_last(range(1, n))
+        pl.when(jnp.logical_not(soon))(lambda: send_last(range(1)))
         for d in range(2, n - 1):
             with jax.named_scope("xr2"):
                 sides(d, xrelay)
@@ -442,10 +449,15 @@
     def step(j, carry):
         with jax.named_scope("yf1_2"):
 
-            @pl.when(at_end & (j < n))
+            @pl.when(at_end & (j == 0))
             def _():
                 for d in range(2, n - 1):
-                    yforward(1, d, piece=j)
+                    yforward(1, d, piece=0)
+
+            @pl.when(at_end & (j < n - 1))
+            def _():
+                for d in range(2, n - 1):
+                    yforward(1, d, piece=j + 1)
 
         @pl.when(j == n - 1)
         def _():
@@ -456,7 +468,13 @@
         c = jnp.where(split, j // (n - 1), lax.rem(j, CHUNKS))
         i = jnp.where(split, lax.rem(j, n - 1), j // CHUNKS)
         with jax.named_scope("comp"):
-            compute(c, i)
+            compute(c, i, inner & (j > 0) & (j < n - 1))
+
+        @pl.when(inner & (j == n - 1))
+        def _():
+            for k in range(1, n - 1):
+                hcopy(0, k, target(k)).start()
+
         return carry
 
     lax.fori_loop(0, n * CHUNKS, step, 0)

time: 53.7 us -> 52.8 us (0.983)
  Pallas kernels: 52.9 us -> 52 us
    pallas_call x1, Pallas kernels: 51.4 us -> 50.6 us  [dense(): pl.pallas_call(functools.partial(dense_kernel, n, nt, width), out_shape=(...]
where the time goes in v5:
time: 52.8 us; the launch traced here: 52.7 us
  Pallas kernels  52 us (98%)
  between operations  0.64 us (1%)
    pallas_call x1, Pallas kernels, dense(): pl.pallas_call(functools.partial(dense_kernel, n, nt, width), out_shape=(...  50.6 us
    pallas_call x1, Pallas kernels, dense(): pl.pallas_call(emit_kernel, out_shape=(jax.ShapeDtypeStruct((1, width, fc...  1.43 us

profile of v5, /device:TPU:0, one launch (start us, length us, event | category | flops | bytes accessed | tf_op | source)
XLA Modules:
  0.0 52.7 jit_solution(4218795944678752659)
XLA Ops:
  0.6 50.6 %shard_map.85 = (bf16[2,2048,256]{2,1,0:T(8,128)(2,1)S(1)}, bf16[4,2,256,128]{3,2,1,0:T(8,128)(2,1)S(1)}, f32[2,256,128]{2,1,0:T(8,128)S(1)}, f32[2,256,128]{2,1,0:T(8,128)S(1)}) custom-call(bf16[256,2048]{1,0:T(8,128)(2,1)} %tok_hbm.1, f32[1,512]{1,0:T(1,128)} %bitcast.3, f32[4,512,256]{2,1,0:T(8,128)} %gate_hbm.1, f32[4,512,256]{2,1,0:T(8,128)} %up_hbm.1, ...), custom_call_target="tpu_custom_call" | custom-call | tf_op jit(solution)/shard_map/pallas_call | solution.py:538
  51.3 1.4 %shard_map.86 = (bf16[1,2048,256]{2,1,0:T(8,128)(2,1)}, bf16[1,2048,256]{2,1,0:T(8,128)(2,1)}, bf16[256,2,256]{2,1,0:T(2,128)(2,1)}) custom-call(bf16[2,2048,256]{2,1,0:T(8,128)(2,1)S(1)} %get-tuple-element.7.served, bf16[4,2,256,128]{3,2,1,0:T(8,128)(2,1)S(1)} %get-tuple-element.8.hr, f32[2,256,128]{2,1,0:T(8,128)S(1)} %get-tuple-element.9.names, ...), custom_call_target="tpu_custom_call" | custom-call | tf_op jit(solution)/shard_map/pallas_call | solution.py:572

commit v6 on v5

--- a/solution.py
+++ b/solution.py
@@ -387,11 +387,11 @@
                 arrive_all(d, (lambda: pl.when(slow)(send_far)) if d == n - 2 else None)
         pl.when(jnp.logical_not(slow))(send_far)
         for d in range(2, n - 1):
+            with jax.named_scope("yf0_2"):
+                yforward(0, d)
+        for d in range(2, n - 1):
             with jax.named_scope("xr2"):
                 sides(d, xrelay)
-        for d in range(2, n - 1):
-            with jax.named_scope("yf0_2"):
-                yforward(0, d)
         with jax.named_scope("arr3a"):
             arrive_half(n - 1, 0)
         for h in range(1, HALVES):
@@ -399,10 +399,10 @@
                 arrive_half(n - 1, h)
         with jax.named_scope("yf0_3"):
             yforward(0, n - 1)
+        with jax.named_scope("yf1_3"):
+            yforward(1, n - 1)
         with jax.named_scope("xr3"):
             sides(n - 1, xrelay)
-        with jax.named_scope("yf1_3"):
-            yforward(1, n - 1)
         totals()
 
     @pl.when(inner)
@@ -591,7 +591,7 @@
     fits = (
         experts == n
         and capacity >= rows
-        and n >= 3
+        and n >= 4
         and nt == 4
         and lax.axis_size("grp") == 2
         and width == nt * depth

time: 52.8 us -> 53.3 us (level)
  no operation moved by 1% of the time
where the time goes in v6:
time: 53.3 us; the launch traced here: 53.2 us
  Pallas kernels  52.5 us (98%)
  between operations  0.64 us (1%)
    pallas_call x1, Pallas kernels, dense(): pl.pallas_call(functools.partial(dense_kernel, n, nt, width), out_shape=(...  51.1 us
    pallas_call x1, Pallas kernels, dense(): pl.pallas_call(emit_kernel, out_shape=(jax.ShapeDtypeStruct((1, width, fc...  1.43 us

profile of v6, /device:TPU:0, one launch (start us, length us, event | category | flops | bytes accessed | tf_op | source)
XLA Modules:
  0.0 53.2 jit_solution(6534571493205204824)
XLA Ops:
  0.6 51.1 %shard_map.85 = (bf16[2,2048,256]{2,1,0:T(8,128)(2,1)S(1)}, bf16[4,2,256,128]{3,2,1,0:T(8,128)(2,1)S(1)}, f32[2,256,128]{2,1,0:T(8,128)S(1)}, f32[2,256,128]{2,1,0:T(8,128)S(1)}) custom-call(bf16[256,2048]{1,0:T(8,128)(2,1)} %tok_hbm.1, f32[1,512]{1,0:T(1,128)} %bitcast.3, f32[4,512,256]{2,1,0:T(8,128)} %gate_hbm.1, f32[4,512,256]{2,1,0:T(8,128)} %up_hbm.1, ...), custom_call_target="tpu_custom_call" | custom-call | tf_op jit(solution)/shard_map/pallas_call | solution.py:538
  51.8 1.4 %shard_map.86 = (bf16[1,2048,256]{2,1,0:T(8,128)(2,1)}, bf16[1,2048,256]{2,1,0:T(8,128)(2,1)}, bf16[256,2,256]{2,1,0:T(2,128)(2,1)}) custom-call(bf16[2,2048,256]{2,1,0:T(8,128)(2,1)S(1)} %get-tuple-element.7.served, bf16[4,2,256,128]{3,2,1,0:T(8,128)(2,1)S(1)} %get-tuple-element.8.hr, f32[2,256,128]{2,1,0:T(8,128)S(1)} %get-tuple-element.9.names, ...), custom_call_target="tpu_custom_call" | custom-call | tf_op jit(solution)/shard_map/pallas_call | solution.py:572

commit v7 on v5

--- a/solution.py
+++ b/solution.py
@@ -591,7 +591,7 @@
     fits = (
         experts == n
         and capacity >= rows
-        and n >= 3
+        and n >= 4
         and nt == 4
         and lax.axis_size("grp") == 2
         and width == nt * depth

time: 52.8 us -> 52.8 us (level)
  no operation moved by 1% of the time
where the time goes in v7:
time: 52.8 us; the launch traced here: 52.7 us
  Pallas kernels  52 us (98%)
  between operations  0.64 us (1%)
    pallas_call x1, Pallas kernels, dense(): pl.pallas_call(functools.partial(dense_kernel, n, nt, width), out_shape=(...  50.6 us
    pallas_call x1, Pallas kernels, dense(): pl.pallas_call(emit_kernel, out_shape=(jax.ShapeDtypeStruct((1, width, fc...  1.43 us

profile of v7, /device:TPU:0, one launch (start us, length us, event | category | flops | bytes accessed | tf_op | source)
XLA Modules:
  0.0 52.7 jit_solution(4218795944678752659)
XLA Ops:
  0.6 50.6 %shard_map.85 = (bf16[2,2048,256]{2,1,0:T(8,128)(2,1)S(1)}, bf16[4,2,256,128]{3,2,1,0:T(8,128)(2,1)S(1)}, f32[2,256,128]{2,1,0:T(8,128)S(1)}, f32[2,256,128]{2,1,0:T(8,128)S(1)}) custom-call(bf16[256,2048]{1,0:T(8,128)(2,1)} %tok_hbm.1, f32[1,512]{1,0:T(1,128)} %bitcast.3, f32[4,512,256]{2,1,0:T(8,128)} %gate_hbm.1, f32[4,512,256]{2,1,0:T(8,128)} %up_hbm.1, ...), custom_call_target="tpu_custom_call" | custom-call | tf_op jit(solution)/shard_map/pallas_call | solution.py:538
  51.3 1.4 %shard_map.86 = (bf16[1,2048,256]{2,1,0:T(8,128)(2,1)}, bf16[1,2048,256]{2,1,0:T(8,128)(2,1)}, bf16[256,2,256]{2,1,0:T(2,128)(2,1)}) custom-call(bf16[2,2048,256]{2,1,0:T(8,128)(2,1)S(1)} %get-tuple-element.7.served, bf16[4,2,256,128]{3,2,1,0:T(8,128)(2,1)S(1)} %get-tuple-element.8.hr, f32[2,256,128]{2,1,0:T(8,128)S(1)} %get-tuple-element.9.names, ...), custom_call_target="tpu_custom_call" | custom-call | tf_op jit(solution)/shard_map/pallas_call | solution.py:572

commit v8 on v7

--- a/solution.py
+++ b/solution.py
@@ -347,7 +347,7 @@
             for c in range(1, CHUNKS):
                 pl.when(here)(functools.partial(send_weights, c, 1, sign))
 
-    soon = z == n - 2
+    soon = (z == n - 2) & (lax.rem(t, 2) == 1)
 
     def send_last(pieces):
         for c in range(1, CHUNKS):
@@ -357,7 +357,7 @@
     with jax.named_scope("arr1"):
         arrive_all(1)
     pl.when(inner)(send_mid)
-    pl.when(inner & soon)(lambda: send_last(range(1)))
+    pl.when(inner & soon)(lambda: send_last(range(2)))
 
     local(
         tok_hbm.at[:, pl.ds(0, (nt - 1) * depth)], tok_hbm.at[:, pl.ds(0, (nt - 1) * depth)], ls_tok
@@ -419,8 +419,8 @@
         for d in range(2, n - 1):
             with jax.named_scope("yf0_2"):
                 yforward(0, d)
-        send_last(range(1, n))
-        pl.when(jnp.logical_not(soon))(lambda: send_last(range(1)))
+        send_last(range(2, n))
+        pl.when(jnp.logical_not(soon))(lambda: send_last(range(2)))
         for d in range(2, n - 1):
             with jax.named_scope("xr2"):
                 sides(d, xrelay)

time: 52.8 us -> 52.5 us (level)
  no operation moved by 1% of the time
where the time goes in v8:
time: 52.5 us; the launch traced here: 52.3 us
  Pallas kernels  51.7 us (98%)
  between operations  0.64 us (1%)
    pallas_call x1, Pallas kernels, dense(): pl.pallas_call(functools.partial(dense_kernel, n, nt, width), out_shape=(...  50.3 us
    pallas_call x1, Pallas kernels, dense(): pl.pallas_call(emit_kernel, out_shape=(jax.ShapeDtypeStruct((1, width, fc...  1.43 us

profile of v8, /device:TPU:0, one launch (start us, length us, event | category | flops | bytes accessed | tf_op | source)
XLA Modules:
  0.0 52.3 jit_solution(12447311598432811919)
XLA Ops:
  0.6 50.3 %shard_map.85 = (bf16[2,2048,256]{2,1,0:T(8,128)(2,1)S(1)}, bf16[4,2,256,128]{3,2,1,0:T(8,128)(2,1)S(1)}, f32[2,256,128]{2,1,0:T(8,128)S(1)}, f32[2,256,128]{2,1,0:T(8,128)S(1)}) custom-call(bf16[256,2048]{1,0:T(8,128)(2,1)} %tok_hbm.1, f32[1,512]{1,0:T(1,128)} %bitcast.3, f32[4,512,256]{2,1,0:T(8,128)} %gate_hbm.1, f32[4,512,256]{2,1,0:T(8,128)} %up_hbm.1, ...), custom_call_target="tpu_custom_call" | custom-call | tf_op jit(solution)/shard_map/pallas_call | solution.py:538
  50.9 1.4 %shard_map.86 = (bf16[1,2048,256]{2,1,0:T(8,128)(2,1)}, bf16[1,2048,256]{2,1,0:T(8,128)(2,1)}, bf16[256,2,256]{2,1,0:T(2,128)(2,1)}) custom-call(bf16[2,2048,256]{2,1,0:T(8,128)(2,1)S(1)} %get-tuple-element.7.served, bf16[4,2,256,128]{3,2,1,0:T(8,128)(2,1)S(1)} %get-tuple-element.8.hr, f32[2,256,128]{2,1,0:T(8,128)S(1)} %get-tuple-element.9.names, ...), custom_call_target="tpu_custom_call" | custom-call | tf_op jit(solution)/shard_map/pallas_call | solution.py:572
